TPU v7x, 32 devices: a whole 2x2x4 slice. The times are simulated.
32 devices in a mesh: grp: 2 (over y), dp: 2 (over x), kv: 4 (over z), tp: 2 (over core).
Axes of the slice: x: 2, y: 2, z: 4, core: 2. Of those that a mesh axis runs over, the one named last changes fastest.
Arguments:
- residual_input: bfloat16 [128, 4096], P(('grp', 'dp', 'tp'), 'kv'), parts along dimension 0, may hold values from -6 to 6
- incoming_state: float32 [128, 16, 64, 128], P(('grp', 'kv'), ('dp', 'tp')), parts along dimension 0, may hold values from -4 to 4
- extra_log_decay: float32 [128, 1024], P(('grp', 'kv'), ('dp', 'tp')), parts along dimension 0, may hold values from -0.7 to 0
- leading_norm_gain: float32 [4096], P('kv'), may hold values from 0.1 to 1.9
- leading_gate_weight: bfloat16 [4096, 11264], P('kv', ('dp', 'tp')), may hold values from -0.09375 to 0.09375
- leading_up_weight: bfloat16 [4096, 11264], P('kv', ('dp', 'tp')), may hold values from -0.09375 to 0.09375
- leading_down_weight: bfloat16 [11264, 4096], P(('dp', 'tp'), 'kv'), may hold values from -0.0546875 to 0.0546875
- attention_norm_gain: float32 [4096], P('kv'), may hold values from 0.1 to 1.9
- query_projector: bfloat16 [4096, 1024], P('kv', ('dp', 'tp')), may hold values from -0.09375 to 0.09375
- key_projector: bfloat16 [4096, 1024], P('kv', ('dp', 'tp')), may hold values from -0.09375 to 0.09375
- value_projector: bfloat16 [4096, 2048], P('kv', ('dp', 'tp')), may hold values from -0.09375 to 0.09375
- output_gate_weight: bfloat16 [4096, 2048], P('kv', ('dp', 'tp')), may hold values from -0.09375 to 0.09375
- forget_weight: bfloat16 [4096, 1024], P('kv', ('dp', 'tp')), may hold values from -0.75 to 0.75
- head_norm_gain: float32 [128], replicated, may hold values from 0.1 to 1.9
- output_projector: bfloat16 [2048, 4096], P(('dp', 'tp'), 'kv'), may hold values from -0.125 to 0.125
- trailing_norm_gain: float32 [4096], P('kv'), may hold values from 0.1 to 1.9
- trailing_gate_weight: bfloat16 [4096, 11264], P('kv', ('dp', 'tp')), may hold values from -0.09375 to 0.09375
- trailing_up_weight: bfloat16 [4096, 11264], P('kv', ('dp', 'tp')), may hold values from -0.09375 to 0.09375
- trailing_down_weight: bfloat16 [11264, 4096], P(('dp', 'tp'), 'kv'), may hold values from -0.0546875 to 0.0546875
Outputs:
- result: bfloat16 [128, 4096], P(('grp', 'dp', 'tp'), 'kv'), parts along dimension 0
- new_state: float32 [128, 16, 64, 128], P(('grp', 'kv'), ('dp', 'tp')), parts along dimension 0
There are 2 independent parts, one for each index of `grp`. A program takes and returns all parts, laid end to end along the dimension named above; an argument that names none is the same for every part. Nothing has to cross between parts.
All inputs are finite; a program needn't handle non-finite values.
Results may differ from a plain program's by a relative error of at most 0.0095.
Values may be sent and summed in bfloat16 or wider, within the bound.
A program may use at most 128 MiB of HBM per device.

v0:
```python
import jax
import jax.numpy as jnp
from jax import lax
from jax.sharding import PartitionSpec as P

D = 4096
KEY_CHANNELS = 64
VALUE_DIM = 128
epsilon = 1e-06


def batch_rows(row_block):
    return lax.all_gather(row_block, ("dp", "tp"), axis=0, tiled=True)


def channel_mixer(row_block, norm_gain, gate_matrix, up_matrix, down_matrix):
    gathered = batch_rows(row_block)
    widened = gathered.astype(jnp.float32)
    squares = jnp.sum(widened * widened, axis=1)
    scaled = (widened * norm_gain).astype(jnp.bfloat16)
    gate_part = jnp.dot(scaled, gate_matrix, preferred_element_type=jnp.float32)
    up_part = jnp.dot(scaled, up_matrix, preferred_element_type=jnp.float32)
    gate_sum, up_sum, row_total = (
        lax.psum_scatter(gate_part, "kv", scatter_dimension=0, tiled=True),
        lax.psum_scatter(up_part, "kv", scatter_dimension=0, tiled=True),
        lax.psum_scatter(squares, "kv", scatter_dimension=0, tiled=True),
    )
    decay_factor = lax.rsqrt(row_total / D + epsilon)[:, None]
    hidden_share = (jax.nn.silu(decay_factor * gate_sum) * (decay_factor * up_sum)).astype(
        jnp.bfloat16
    )
    hidden = lax.all_gather(hidden_share, "kv", axis=0, tiled=True)
    return lax.psum_scatter(
        jnp.dot(hidden, down_matrix, preferred_element_type=jnp.float32),
        ("dp", "tp"),
        scatter_dimension=0,
        tiled=True,
    )


def per_device(
    residual_input,
    incoming_state,
    extra_log_decay,
    leading_norm_gain,
    leading_gate_weight,
    leading_up_weight,
    leading_down_weight,
    attention_norm_gain,
    query_projector,
    key_projector,
    value_projector,
    output_gate_weight,
    forget_weight,
    head_norm_gain,
    output_projector,
    trailing_norm_gain,
    trailing_gate_weight,
    trailing_up_weight,
    trailing_down_weight,
):
    after_first = (
        residual_input.astype(jnp.float32)
        + 0.5
        * channel_mixer(
            residual_input,
            leading_norm_gain,
            leading_gate_weight,
            leading_up_weight,
            leading_down_weight,
        )
    ).astype(jnp.bfloat16)
    gathered = batch_rows(after_first)
    widened = gathered.astype(jnp.float32)
    squares = jnp.sum(widened * widened, axis=1)
    scaled = (widened * attention_norm_gain).astype(jnp.bfloat16)
    query_part = jnp.dot(scaled, query_projector, preferred_element_type=jnp.float32)
    key_part = jnp.dot(scaled, key_projector, preferred_element_type=jnp.float32)
    value_part = jnp.dot(scaled, value_projector, preferred_element_type=jnp.float32)
    gate_part = jnp.dot(scaled, output_gate_weight, preferred_element_type=jnp.float32)
    decay_part = jnp.dot(scaled, forget_weight, preferred_element_type=jnp.float32)
    query_sum, key_sum, value_sum, gate_sum, decay_total, row_total = (
        lax.psum_scatter(query_part, "kv", scatter_dimension=0, tiled=True),
        lax.psum_scatter(key_part, "kv", scatter_dimension=0, tiled=True),
        lax.psum_scatter(value_part, "kv", scatter_dimension=0, tiled=True),
        lax.psum_scatter(gate_part, "kv", scatter_dimension=0, tiled=True),
        lax.psum_scatter(decay_part, "kv", scatter_dimension=0, tiled=True),
        lax.psum_scatter(squares, "kv", scatter_dimension=0, tiled=True),
    )
    decay_factor = lax.rsqrt(row_total / D + epsilon)[:, None]
    row_count = query_sum.shape[0]
    heads_here = query_sum.shape[1] // KEY_CHANNELS
    queries = (decay_factor * query_sum).reshape(
        row_count, heads_here, KEY_CHANNELS
    ) * KEY_CHANNELS ** (-0.5)
    key_rows = (decay_factor * key_sum).reshape(row_count, heads_here, KEY_CHANNELS)
    value_rows = (decay_factor * value_sum).reshape(row_count, heads_here, VALUE_DIM)
    gate_rows = (decay_factor * gate_sum).reshape(row_count, heads_here, VALUE_DIM)
    decay_logarithm = (
        jax.nn.log_sigmoid(decay_factor * decay_total) / 16.0 + extra_log_decay
    ).reshape(row_count, heads_here, KEY_CHANNELS)
    new_state = (
        jnp.exp(decay_logarithm)[..., None] * incoming_state
        + key_rows[..., None] * value_rows[:, :, None, :]
    )
    read_out = jnp.einsum("bhk,bhkv->bhv", queries, new_state, precision=lax.Precision.HIGHEST)
    normed = read_out * lax.rsqrt(jnp.mean(read_out * read_out, axis=-1, keepdims=True) + epsilon)
    head_rows = (
        (normed * head_norm_gain * jax.nn.silu(gate_rows))
        .astype(jnp.bfloat16)
        .reshape(row_count, heads_here * VALUE_DIM)
    )
    all_heads = lax.all_gather(head_rows, "kv", axis=0, tiled=True)
    mixed_rows = lax.psum_scatter(
        jnp.dot(all_heads, output_projector, preferred_element_type=jnp.float32),
        ("dp", "tp"),
        scatter_dimension=0,
        tiled=True,
    )
    second = (after_first.astype(jnp.float32) + mixed_rows).astype(jnp.bfloat16)
    result = (
        second.astype(jnp.float32)
        + 0.5
        * channel_mixer(
            second,
            trailing_norm_gain,
            trailing_gate_weight,
            trailing_up_weight,
            trailing_down_weight,
        )
    ).astype(jnp.bfloat16)
    return (result, new_state)


def solution(mesh):
    return jax.shard_map(
        per_device,
        mesh=mesh,
        in_specs=(
            P(("grp", "dp", "tp"), "kv"),
            P(("grp", "kv"), ("dp", "tp"), None, None),
            P(("grp", "kv"), ("dp", "tp")),
            P("kv"),
            P("kv", ("dp", "tp")),
            P("kv", ("dp", "tp")),
            P(("dp", "tp"), "kv"),
            P("kv"),
            P("kv", ("dp", "tp")),
            P("kv", ("dp", "tp")),
            P("kv", ("dp", "tp")),
            P("kv", ("dp", "tp")),
            P("kv", ("dp", "tp")),
            P(),
            P(("dp", "tp"), "kv"),
            P("kv"),
            P("kv", ("dp", "tp")),
            P("kv", ("dp", "tp")),
            P(("dp", "tp"), "kv"),
        ),
        out_specs=(P(("grp", "dp", "tp"), "kv"), P(("grp", "kv"), ("dp", "tp"), None, None)),
        check_vma=False,
    )
```

profile of v0, /device:TPU:0, one launch (start us, length us, event | category | flops | bytes accessed | tf_op | source)
XLA Modules:
  0.0 359.7 jit_solution(16201497556303995588)
XLA Ops:
  7.2 6.9 %all_gather.18 = bf16[64,1024]{1,0:T(8,128)(2,1)S(1)} all-gather(bf16[16,1024]{1,0:T(8,128)(2,1)} %param.19), channel_id=1, replica_groups=mesh['grp'=2,'dp'=2,'kv'=4,'tp'=2] {'dp','tp'}, dimensions={0}, use_global_device_ids=true | all-gather | bytes 163840 | tf_op jit(solution)/shard_map/all_gather | solution.py:13
  14.1 4.6 %fusion.10 = f32[64,2816]{1,0:T(8,128)} fusion(bf16[1024,2816]{1,0:T(8,128)(2,1)} %param.24, bf16[64,1024]{1,0:T(8,128)(2,1)S(1)} %all_gather.18, f32[1024]{0:T(1024)} %param.22), kind=kOutput, calls=%fused_computation.17 | convolution fusion | flops 369295360 | bytes 6623232 | tf_op jit(solution)/shard_map/dot_general | solution.py:22
  18.8 4.6 %fusion.12 = f32[64,2816]{1,0:T(8,128)} fusion(bf16[1024,2816]{1,0:T(8,128)(2,1)} %param.23, bf16[64,1024]{1,0:T(8,128)(2,1)S(1)} %all_gather.18, f32[1024]{0:T(1024)S(1)} %copy-done.7), kind=kOutput, calls=%fused_computation.18 | convolution fusion | flops 369295360 | bytes 6623232 | tf_op jit(solution)/shard_map/dot_general | solution.py:21
  24.9 12.7 %all-reduce = f32[64]{0:T(128)S(1)} all-reduce(f32[64]{0:T(128)S(1)} %fusion), channel_id=2, replica_groups=mesh['grp'=2,'dp'=2,'kv'=4,'tp'=2] {'kv'}, use_global_device_ids=true, to_apply=%region_1.0.clone | all-reduce | flops 64 | bytes 512
  37.6 6.1 %reduce-scatter.15.cloned.1.call-done = f32[16,2816]{1,0:T(8,128)} async-done(((f32[64,2816]{1,0:T(8,128)}), f32[16,2816]{1,0:T(8,128)}) %reduce-scatter.15.cloned.1.call-update) | async-done | bytes 180240 | tf_op jit(solution)/shard_map/reduce_scatter | solution.py:25
  43.7 24.4 %reduce-scatter.13.cloned.1.call-done = f32[16,2816]{1,0:T(8,128)} async-done(((f32[64,2816]{1,0:T(8,128)}), f32[16,2816]{1,0:T(8,128)}) %reduce-scatter.13.cloned.1.call-update) | async-done | bytes 180240 | tf_op jit(solution)/shard_map/reduce_scatter | solution.py:24
  69.3 15.1 %all_gather.19 = bf16[64,2816]{1,0:T(8,128)(2,1)S(1)} all-gather(bf16[16,2816]{1,0:T(8,128)(2,1)S(1)} %multiply_convert_fusion.1), channel_id=1, replica_groups=mesh['grp'=2,'dp'=2,'kv'=4,'tp'=2] {'kv'}, dimensions={0}, use_global_device_ids=true | all-gather | bytes 450560 | tf_op jit(solution)/shard_map/all_gather | solution.py:32
  84.4 4.5 %fusion.36 = f32[64,1024]{1,0:T(8,128)} fusion(bf16[64,2816]{1,0:T(8,128)(2,1)S(1)} %all_gather.19, bf16[2816,1024]{1,0:T(8,128)(2,1)} %param.25), kind=kOutput, calls=%fused_computation.51 | convolution fusion | flops 369098752 | bytes 6389760 | tf_op jit(solution)/shard_map/dot_general | solution.py:34
  88.9 19.0 %reduce-scatter.17.cloned.1.call-done = f32[16,1024]{1,0:T(8,128)} async-done(((f32[64,1024]{1,0:T(8,128)}), f32[16,1024]{1,0:T(8,128)}) %reduce-scatter.17.cloned.1.call-update) | async-done | bytes 65552 | tf_op jit(solution)/shard_map/reduce_scatter | solution.py:33
  108.8 5.4 %all_gather.20 = bf16[64,1024]{1,0:T(8,128)(2,1)S(1)} all-gather(bf16[16,1024]{1,0:T(8,128)(2,1)S(1)} %add_convert_fusion.2), channel_id=1, replica_groups=mesh['grp'=2,'dp'=2,'kv'=4,'tp'=2] {'dp','tp'}, dimensions={0}, use_global_device_ids=true | all-gather | bytes 163840 | tf_op jit(solution)/shard_map/all_gather | solution.py:13
  114.3 1.9 fusion.20
  116.2 1.9 fusion.18
  118.2 1.9 fusion.22
  121.3 11.8 %all-reduce.1 = f32[64]{0:T(128)S(1)} all-reduce(f32[64]{0:T(128)S(1)} %fusion.2), channel_id=6, replica_groups=mesh['grp'=2,'dp'=2,'kv'=4,'tp'=2] {'kv'}, use_global_device_ids=true, to_apply=%region_6.7.clone | all-reduce | flops 64 | bytes 512
  134.1 1.5 reduce-scatter.21.cloned.1.call-done
  135.6 19.5 %reduce-scatter.23.cloned.1.call-done = f32[16,256]{1,0:T(8,128)} async-done(((f32[64,256]{1,0:T(8,128)}), f32[16,256]{1,0:T(8,128)}) %reduce-scatter.23.cloned.1.call-update) | async-done | bytes 16400 | tf_op jit(solution)/shard_map/reduce_scatter | solution.py:84
  155.2 19.6 %reduce-scatter.19.cloned.1.call-done = f32[16,256]{1,0:T(8,128)} async-done(((f32[64,256]{1,0:T(8,128)}), f32[16,256]{1,0:T(8,128)}) %reduce-scatter.19.cloned.1.call-update) | async-done | bytes 16400 | tf_op jit(solution)/shard_map/reduce_scatter | solution.py:83
  175.9 18.8 %reduce-scatter.27.cloned.1.call-done = f32[16,512]{1,0:T(8,128)} async-done(((f32[64,512]{1,0:T(8,128)}), f32[16,512]{1,0:T(8,128)}) %reduce-scatter.27.cloned.1.call-update) | async-done | bytes 32784 | tf_op jit(solution)/shard_map/reduce_scatter | solution.py:86
  194.7 20.5 %reduce-scatter.25.cloned.1.call-done = f32[16,512]{1,0:T(8,128)} async-done(((f32[64,512]{1,0:T(8,128)}), f32[16,512]{1,0:T(8,128)}) %reduce-scatter.25.cloned.1.call-update) | async-done | bytes 32784 | tf_op jit(solution)/shard_map/reduce_scatter | solution.py:85
  216.0 2.5 multiply_add_fusion
  218.5 1.9 fusion.37
  220.6 13.1 %all_gather.21 = bf16[64,512]{1,0:T(8,128)(2,1)S(1)} all-gather(bf16[16,512]{1,0:T(8,128)(2,1)S(1)} %bitcast.28), channel_id=1, replica_groups=mesh['grp'=2,'dp'=2,'kv'=4,'tp'=2] {'kv'}, dimensions={0}, use_global_device_ids=true | all-gather | bytes 81920 | tf_op jit(solution)/shard_map/all_gather | solution.py:113
  234.8 18.3 %reduce-scatter.29.cloned.1.call-done = f32[16,1024]{1,0:T(8,128)} async-done(((f32[64,1024]{1,0:T(8,128)}), f32[16,1024]{1,0:T(8,128)}) %reduce-scatter.29.cloned.1.call-update) | async-done | bytes 65552 | tf_op jit(solution)/shard_map/reduce_scatter | solution.py:114
  254.0 5.4 %all_gather.22 = bf16[64,1024]{1,0:T(8,128)(2,1)S(1)} all-gather(bf16[16,1024]{1,0:T(8,128)(2,1)S(1)} %add_convert_fusion.1), channel_id=1, replica_groups=mesh['grp'=2,'dp'=2,'kv'=4,'tp'=2] {'dp','tp'}, dimensions={0}, use_global_device_ids=true | all-gather | bytes 163840 | tf_op jit(solution)/shard_map/all_gather | solution.py:13
  259.4 4.6 %fusion.6 = f32[64,2816]{1,0:T(8,128)} fusion(bf16[1024,2816]{1,0:T(8,128)(2,1)} %param.36, bf16[64,1024]{1,0:T(8,128)(2,1)S(1)} %all_gather.22, f32[1024]{0:T(1024)S(1)} %copy-done.8), kind=kOutput, calls=%fused_computation.15 | convolution fusion | flops 369295360 | bytes 6623232 | tf_op jit(solution)/shard_map/dot_general | solution.py:22
  264.1 4.6 %fusion.8 = f32[64,2816]{1,0:T(8,128)} fusion(bf16[1024,2816]{1,0:T(8,128)(2,1)} %param.35, bf16[64,1024]{1,0:T(8,128)(2,1)S(1)} %all_gather.22, f32[1024]{0:T(1024)S(1)} %copy-done.8), kind=kOutput, calls=%fused_computation.16 | convolution fusion | flops 369295360 | bytes 6623232 | tf_op jit(solution)/shard_map/dot_general | solution.py:21
  268.9 12.0 %all-reduce.2 = f32[64]{0:T(128)S(1)} all-reduce(f32[64]{0:T(128)S(1)} %fusion.4), channel_id=13, replica_groups=mesh['grp'=2,'dp'=2,'kv'=4,'tp'=2] {'kv'}, use_global_device_ids=true, to_apply=%region_15.16.clone | all-reduce | flops 64 | bytes 512
  281.0 6.4 %reduce-scatter.33.cloned.1.call-done = f32[16,2816]{1,0:T(8,128)} async-done(((f32[64,2816]{1,0:T(8,128)}), f32[16,2816]{1,0:T(8,128)}) %reduce-scatter.33.cloned.1.call-update) | async-done | bytes 180240 | tf_op jit(solution)/shard_map/reduce_scatter | solution.py:25
  287.4 24.3 %reduce-scatter.31.cloned.1.call-done = f32[16,2816]{1,0:T(8,128)} async-done(((f32[64,2816]{1,0:T(8,128)}), f32[16,2816]{1,0:T(8,128)}) %reduce-scatter.31.cloned.1.call-update) | async-done | bytes 180240 | tf_op jit(solution)/shard_map/reduce_scatter | solution.py:24
  312.8 14.9 %all_gather.23 = bf16[64,2816]{1,0:T(8,128)(2,1)S(1)} all-gather(bf16[16,2816]{1,0:T(8,128)(2,1)S(1)} %multiply_convert_fusion), channel_id=1, replica_groups=mesh['grp'=2,'dp'=2,'kv'=4,'tp'=2] {'kv'}, dimensions={0}, use_global_device_ids=true | all-gather | bytes 450560 | tf_op jit(solution)/shard_map/all_gather | solution.py:32
  327.7 4.5 %fusion.39 = f32[64,1024]{1,0:T(8,128)} fusion(bf16[64,2816]{1,0:T(8,128)(2,1)S(1)} %all_gather.23, bf16[2816,1024]{1,0:T(8,128)(2,1)} %param.37), kind=kOutput, calls=%fused_computation.54 | convolution fusion | flops 369098752 | bytes 6389760 | tf_op jit(solution)/shard_map/dot_general | solution.py:34
  332.2 19.2 %reduce-scatter.35.cloned.1.call-done = f32[16,1024]{1,0:T(8,128)} async-done(((f32[64,1024]{1,0:T(8,128)}), f32[16,1024]{1,0:T(8,128)}) %reduce-scatter.35.cloned.1.call-update) | async-done | bytes 65552 | tf_op jit(solution)/shard_map/reduce_scatter | solution.py:33
  (72 shorter events, 12.4 us)
Async XLA Ops:
  7.2 226.6 %copy-start = (bf16[512,1024]{1,0:T(8,128)(2,1)S(1)}, bf16[512,1024]{1,0:T(8,128)(2,1)}, u32[]{:S(2)}) copy-start(bf16[512,1024]{1,0:T(8,128)(2,1)} %param.33) | copy-start | bytes 3145732
  7.2 11.6 %copy-start.7 = (f32[1024]{0:T(1024)S(1)}, f32[1024]{0:T(1024)}, u32[]{:S(2)}) copy-start(f32[1024]{0:T(1024)} %param.22) | copy-start | bytes 12292
  7.2 36.5 %reduce-scatter.15.cloned.1.call-start = ((), (), s32[]{:S(2)}) async-start(), calls=%async_computation.13 | async-start | bytes 901120 | tf_op jit(solution)/shard_map/reduce_scatter | solution.py:25
  14.1 9.4 %copy-start.10 = (u32[32]{0:T(128)S(1)}, u32[32]{0:T(128)}, u32[]{:S(2)}) copy-start(u32[32]{0:T(128)} %constant.31) | copy-start | bytes 388
  18.8 49.4 %reduce-scatter.13.cloned.1.call-start = ((), (), s32[]{:S(2)}) async-start(), calls=%async_computation.12 | async-start | bytes 901120 | tf_op jit(solution)/shard_map/reduce_scatter | solution.py:24
  23.4 84.5 %copy-start.4 = (bf16[16,1024]{1,0:T(8,128)(2,1)S(1)}, bf16[16,1024]{1,0:T(8,128)(2,1)}, u32[]{:S(2)}) copy-start(bf16[16,1024]{1,0:T(8,128)(2,1)} %param.19) | copy-start | bytes 98308
  23.4 90.8 %copy-start.5 = (f32[1024]{0:T(1024)S(1)}, f32[1024]{0:T(1024)}, u32[]{:S(2)}) copy-start(f32[1024]{0:T(1024)} %param.26) | copy-start | bytes 12292
  23.4 96.7 %copy-start.2 = (bf16[1024,512]{1,0:T(8,128)(2,1)S(1)}, bf16[1024,512]{1,0:T(8,128)(2,1)}, u32[]{:S(2)}) copy-start(bf16[1024,512]{1,0:T(8,128)(2,1)} %param.30) | copy-start | bytes 3145732
  23.5 84.5 %reduce-scatter.17.cloned.1.call-start = ((), (), s32[]{:S(2)}) async-start(), calls=%async_computation.14 | async-start | bytes 327680 | tf_op jit(solution)/shard_map/reduce_scatter | solution.py:33
  69.3 63.8 %copy-start.3 = (bf16[1024,512]{1,0:T(8,128)(2,1)S(1)}, bf16[1024,512]{1,0:T(8,128)(2,1)}, u32[]{:S(2)}) copy-start(bf16[1024,512]{1,0:T(8,128)(2,1)} %param.29) | copy-start | bytes 3145732
  84.4 90.4 %copy-start.6 = (f32[16,256]{1,0:T(8,128)S(1)}, f32[16,256]{1,0:T(8,128)}, u32[]{:S(2)}) copy-start(f32[16,256]{1,0:T(8,128)} %param.21) | copy-start | bytes 49156
  88.9 46.8 %reduce-scatter.21.cloned.1.call-start = ((), (), s32[]{:S(2)}) async-start(), calls=%async_computation.16 | async-start | bytes 81920 | tf_op jit(solution)/shard_map/reduce_scatter | solution.py:87
  116.2 104.3 %copy-start.9 = (f32[128]{0:T(128)S(1)}, f32[128]{0:T(128)}, u32[]{:S(2)}) copy-start(f32[128]{0:T(128)} %param.32) | copy-start | bytes 1540
  116.2 39.0 %reduce-scatter.23.cloned.1.call-start = ((), (), s32[]{:S(2)}) async-start(), calls=%async_computation.17 | async-start | bytes 81920 | tf_op jit(solution)/shard_map/reduce_scatter | solution.py:84
  118.1 56.6 %reduce-scatter.19.cloned.1.call-start = ((), (), s32[]{:S(2)}) async-start(), calls=%async_computation.15 | async-start | bytes 81920 | tf_op jit(solution)/shard_map/reduce_scatter | solution.py:83
  120.1 74.6 %reduce-scatter.27.cloned.1.call-start = ((), (), s32[]{:S(2)}) async-start(), calls=%async_computation.19 | async-start | bytes 163840 | tf_op jit(solution)/shard_map/reduce_scatter | solution.py:86
  121.1 138.3 %copy-start.8 = (f32[1024]{0:T(1024)S(1)}, f32[1024]{0:T(1024)}, u32[]{:S(2)}) copy-start(f32[1024]{0:T(1024)} %param.34) | copy-start | bytes 12292
  121.1 94.1 %reduce-scatter.25.cloned.1.call-start = ((), (), s32[]{:S(2)}) async-start(), calls=%async_computation.18 | async-start | bytes 163840 | tf_op jit(solution)/shard_map/reduce_scatter | solution.py:85
  134.0 119.1 %reduce-scatter.29.cloned.1.call-start = ((), (), s32[]{:S(2)}) async-start(), calls=%async_computation.20 | async-start | bytes 327680 | tf_op jit(solution)/shard_map/reduce_scatter | solution.py:114
  218.5 45.5 %copy-start.1 = (f32[16,4,64,128]{3,2,1,0:T(8,128)}, f32[16,4,64,128]{3,2,1,0:T(8,128)S(1)}, u32[]{:S(2)}) copy-start(f32[16,4,64,128]{3,2,1,0:T(8,128)S(1)} %multiply_add_fusion) | copy-start | bytes 6291460
  234.7 52.6 %reduce-scatter.33.cloned.1.call-start = ((), (), s32[]{:S(2)}) async-start(), calls=%async_computation.22 | async-start | bytes 901120 | tf_op jit(solution)/shard_map/reduce_scatter | solution.py:25
  264.0 47.6 %reduce-scatter.31.cloned.1.call-start = ((), (), s32[]{:S(2)}) async-start(), calls=%async_computation.21 | async-start | bytes 901120 | tf_op jit(solution)/shard_map/reduce_scatter | solution.py:24
  268.7 82.7 %reduce-scatter.35.cloned.1.call-start = ((), (), s32[]{:S(2)}) async-start(), calls=%async_computation.23 | async-start | bytes 327680 | tf_op jit(solution)/shard_map/reduce_scatter | solution.py:33
Sparse Core Ops, SparseCore 0:
  18.9 24.7 reduce-scatter.14
  46.0 22.0 reduce-scatter.12
  89.0 18.9 reduce-scatter.16
  116.3 19.3 reduce-scatter.20
  137.7 17.4 reduce-scatter.22
  157.3 17.4 reduce-scatter.18
  177.0 17.6 reduce-scatter.26
  197.5 17.6 reduce-scatter.24
  234.9 18.2 reduce-scatter.28
  264.1 23.1 reduce-scatter.32
  289.7 21.9 reduce-scatter.30
  332.3 18.9 reduce-scatter.34
where the time goes:
time: 361 us; the launch traced here: 360 us
  waiting for transfers between devices  198 us (55%)
  blocking collectives  97.3 us (27%)
  matrix products  37.8 us (10%)
  between operations  15 us (4%)
  other arithmetic  10.4 us (3%)
    reduce_scatter x2, waiting for transfers between devices, channel_mixer(): lax.psum_scatter(gate_part, 'kv', scatter_dimension=0, tiled=True)  48.7 us
    reduce_scatter x2, waiting for transfers between devices, channel_mixer(): lax.psum_scatter(jnp.dot(hidden, down_matrix, preferred_element_type=jnp....  38.2 us
    unnamed x3, blocking collectives  36.4 us
    all_gather x2, blocking collectives, channel_mixer(): hidden = lax.all_gather(hidden_share, 'kv', axis=0, tiled=True)  30 us
    reduce_scatter x1, waiting for transfers between devices, per_device(): lax.psum_scatter(value_part, 'kv', scatter_dimension=0, tiled=True)  20.5 us
    reduce_scatter x1, waiting for transfers between devices, per_device(): lax.psum_scatter(query_part, 'kv', scatter_dimension=0, tiled=True)  19.6 us
    reduce_scatter x1, waiting for transfers between devices, per_device(): lax.psum_scatter(key_part, 'kv', scatter_dimension=0, tiled=True)  19.5 us
    reduce_scatter x1, waiting for transfers between devices, per_device(): lax.psum_scatter(gate_part, 'kv', scatter_dimension=0, tiled=True)  18.8 us
  transfers between devices with their start and end apart: 12, of which 12 were waited for; matrix products, arithmetic and copies ran while one was open for 5% of the time, Pallas kernels for 0%

commit v1 on v0

--- a/solution.py
+++ b/solution.py
@@ -29,7 +29,12 @@
     hidden_share = (jax.nn.silu(decay_factor * gate_sum) * (decay_factor * up_sum)).astype(
         jnp.bfloat16
     )
-    hidden = lax.all_gather(hidden_share, "kv", axis=0, tiled=True)
+    ring = [hidden_share]
+    for hop in range(3):
+        ring.append(lax.ppermute(ring[-1], "kv", [(dev, (dev + 1) % 4) for dev in range(4)]))
+    hidden = jnp.roll(
+        jnp.concatenate(ring[::-1], axis=0), (lax.axis_index("kv") + 1) * ring[0].shape[0], axis=0
+    )
     return lax.psum_scatter(
         jnp.dot(hidden, down_matrix, preferred_element_type=jnp.float32),
         ("dp", "tp"),

time: 361 us -> 369 us (1.022)
  waiting for transfers between devices: 198 us -> 235 us
  blocking collectives: 97.3 us -> 67.3 us
    ppermute x0 -> x6, waiting for transfers between devices: none -> 38.9 us  [channel_mixer(): lax.ppermute(ring[-1], 'kv', [(dev, (dev + 1) % 4) for dev in range(4)])]
    all_gather x2 -> x0, blocking collectives: 30 us -> none  [channel_mixer(): hidden = lax.all_gather(hidden_share, 'kv', axis=0, tiled=True)]
  transfers between devices with their start and end apart: 12 -> 18, of which waited for: 12 -> 18; matrix products, arithmetic and copies ran while one was open for 5% -> 5% of each run, Pallas kernels for 0% -> 0%
where the time goes in v1:
time: 369 us; the launch traced here: 368 us
  waiting for transfers between devices  235 us (64%)
  blocking collectives  67.3 us (18%)
  matrix products  38.6 us (10%)
  between operations  15 us (4%)
  other arithmetic  10.4 us (3%)
    reduce_scatter x2, waiting for transfers between devices, channel_mixer(): lax.psum_scatter(gate_part, 'kv', scatter_dimension=0, tiled=True)  48.8 us
    ppermute x6, waiting for transfers between devices, channel_mixer(): lax.ppermute(ring[-1], 'kv', [(dev, (dev + 1) % 4) for dev in range(4)])  38.9 us
    reduce_scatter x2, waiting for transfers between devices, channel_mixer(): lax.psum_scatter(jnp.dot(hidden, down_matrix, preferred_element_type=jnp....  36.6 us
    unnamed x3, blocking collectives  36.4 us
    reduce_scatter x1, waiting for transfers between devices, per_device(): lax.psum_scatter(value_part, 'kv', scatter_dimension=0, tiled=True)  20.4 us
    reduce_scatter x1, waiting for transfers between devices, per_device(): lax.psum_scatter(key_part, 'kv', scatter_dimension=0, tiled=True)  19.6 us
    reduce_scatter x1, waiting for transfers between devices, per_device(): lax.psum_scatter(query_part, 'kv', scatter_dimension=0, tiled=True)  19.6 us
    reduce_scatter x1, waiting for transfers between devices, per_device(): lax.psum_scatter(gate_part, 'kv', scatter_dimension=0, tiled=True)  18.8 us
  transfers between devices with their start and end apart: 18, of which 18 were waited for; matrix products, arithmetic and copies ran while one was open for 5% of the time, Pallas kernels for 0%

profile of v1, /device:TPU:0, one launch (start us, length us, event | category | flops | bytes accessed | tf_op | source)
XLA Modules:
  0.0 368.0 jit_solution(7678598062760464416)
XLA Ops:
  7.2 6.9 %all_gather.12 = bf16[64,1024]{1,0:T(8,128)(2,1)S(1)} all-gather(bf16[16,1024]{1,0:T(8,128)(2,1)} %param.21), channel_id=1, replica_groups=mesh['grp'=2,'dp'=2,'kv'=4,'tp'=2] {'dp','tp'}, dimensions={0}, use_global_device_ids=true | all-gather | bytes 163840 | tf_op jit(solution)/shard_map/all_gather | solution.py:13
  14.1 4.6 %fusion.30 = f32[64,2816]{1,0:T(8,128)} fusion(bf16[1024,2816]{1,0:T(8,128)(2,1)} %param.26, bf16[64,1024]{1,0:T(8,128)(2,1)S(1)} %all_gather.12, f32[1024]{0:T(1024)} %param.24), kind=kOutput, calls=%fused_computation.49 | convolution fusion | flops 369295360 | bytes 6623232 | tf_op jit(solution)/shard_map/dot_general | solution.py:22
  18.8 4.6 %fusion.32 = f32[64,2816]{1,0:T(8,128)} fusion(bf16[1024,2816]{1,0:T(8,128)(2,1)} %param.25, bf16[64,1024]{1,0:T(8,128)(2,1)S(1)} %all_gather.12, f32[1024]{0:T(1024)S(1)} %copy-done.7), kind=kOutput, calls=%fused_computation.50 | convolution fusion | flops 369295360 | bytes 6623232 | tf_op jit(solution)/shard_map/dot_general | solution.py:21
  24.9 12.7 %all-reduce = f32[64]{0:T(128)S(1)} all-reduce(f32[64]{0:T(128)S(1)} %fusion.20), channel_id=2, replica_groups=mesh['grp'=2,'dp'=2,'kv'=4,'tp'=2] {'kv'}, use_global_device_ids=true, to_apply=%region_1.0.clone | all-reduce | flops 64 | bytes 512
  37.7 6.0 %reduce-scatter.15.cloned.1.call-done = f32[16,2816]{1,0:T(8,128)} async-done(((f32[64,2816]{1,0:T(8,128)}), f32[16,2816]{1,0:T(8,128)}) %reduce-scatter.15.cloned.1.call-update) | async-done | bytes 180240 | tf_op jit(solution)/shard_map/reduce_scatter | solution.py:25
  43.7 24.4 %reduce-scatter.13.cloned.1.call-done = f32[16,2816]{1,0:T(8,128)} async-done(((f32[64,2816]{1,0:T(8,128)}), f32[16,2816]{1,0:T(8,128)}) %reduce-scatter.13.cloned.1.call-update) | async-done | bytes 180240 | tf_op jit(solution)/shard_map/reduce_scatter | solution.py:24
  69.3 6.3 %collective-permute-done = bf16[16,2816]{1,0:T(8,128)(2,1)S(1)} collective-permute-done((bf16[16,2816]{1,0:T(8,128)(2,1)S(1)}, bf16[16,2816]{1,0:T(8,128)(2,1)S(1)}, u32[]{:S(2)}, u32[]{:S(2)}) %collective-permute-start) | collective-permute-done | bytes 90144 | tf_op jit(solution)/shard_map/ppermute | solution.py:34
  75.6 6.7 %collective-permute-done.1 = bf16[16,2816]{1,0:T(8,128)(2,1)S(1)} collective-permute-done((bf16[16,2816]{1,0:T(8,128)(2,1)S(1)}, bf16[16,2816]{1,0:T(8,128)(2,1)S(1)}, u32[]{:S(2)}, u32[]{:S(2)}) %collective-permute-start.1) | collective-permute-done | bytes 90144 | tf_op jit(solution)/shard_map/ppermute | solution.py:34
  82.4 6.4 %collective-permute-done.2 = bf16[16,2816]{1,0:T(8,128)(2,1)} collective-permute-done((bf16[16,2816]{1,0:T(8,128)(2,1)S(1)}, bf16[16,2816]{1,0:T(8,128)(2,1)}, u32[]{:S(2)}, u32[]{:S(2)}) %collective-permute-start.2) | collective-permute-done | bytes 90144 | tf_op jit(solution)/shard_map/ppermute | solution.py:34
  88.8 4.9 %fusion.14 = f32[64,1024]{1,0:T(8,128)} fusion(bf16[2816,1024]{1,0:T(8,128)(2,1)} %param.27, s32[]{:T(128)S(6)} %select_n.19, bf16[16,2816]{1,0:T(8,128)(2,1)} %collective-permute-done.2, bf16[16,2816]{1,0:T(8,128)(2,1)S(1)} %collective-permute-done.1, bf16[16,2816]{1,0:T(8,128)(2,1)S(1)} %collective-permute-done, ...), kind=kOutput, calls=%fused_computation.29 | convolution fusion | flops 371982336 | bytes 6389764 | tf_op jit(solution)/shard_map/dot_general | solution.py:39
  93.8 18.2 %reduce-scatter.17.cloned.1.call-done = f32[16,1024]{1,0:T(8,128)} async-done(((f32[64,1024]{1,0:T(8,128)}), f32[16,1024]{1,0:T(8,128)}) %reduce-scatter.17.cloned.1.call-update) | async-done | bytes 65552 | tf_op jit(solution)/shard_map/reduce_scatter | solution.py:38
  112.8 5.4 %all_gather.13 = bf16[64,1024]{1,0:T(8,128)(2,1)S(1)} all-gather(bf16[16,1024]{1,0:T(8,128)(2,1)S(1)} %add_convert_fusion.2), channel_id=1, replica_groups=mesh['grp'=2,'dp'=2,'kv'=4,'tp'=2] {'dp','tp'}, dimensions={0}, use_global_device_ids=true | all-gather | bytes 163840 | tf_op jit(solution)/shard_map/all_gather | solution.py:13
  120.2 1.9 fusion.38
  125.3 11.7 %all-reduce.1 = f32[64]{0:T(128)S(1)} all-reduce(f32[64]{0:T(128)S(1)} %fusion.22), channel_id=6, replica_groups=mesh['grp'=2,'dp'=2,'kv'=4,'tp'=2] {'kv'}, use_global_device_ids=true, to_apply=%region_6.8.clone | all-reduce | flops 64 | bytes 512
  139.6 19.6 %reduce-scatter.23.cloned.1.call-done = f32[16,256]{1,0:T(8,128)} async-done(((f32[64,256]{1,0:T(8,128)}), f32[16,256]{1,0:T(8,128)}) %reduce-scatter.23.cloned.1.call-update) | async-done | bytes 16400 | tf_op jit(solution)/shard_map/reduce_scatter | solution.py:89
  159.2 19.6 %reduce-scatter.19.cloned.1.call-done = f32[16,256]{1,0:T(8,128)} async-done(((f32[64,256]{1,0:T(8,128)}), f32[16,256]{1,0:T(8,128)}) %reduce-scatter.19.cloned.1.call-update) | async-done | bytes 16400 | tf_op jit(solution)/shard_map/reduce_scatter | solution.py:88
  179.9 18.8 %reduce-scatter.27.cloned.1.call-done = f32[16,512]{1,0:T(8,128)} async-done(((f32[64,512]{1,0:T(8,128)}), f32[16,512]{1,0:T(8,128)}) %reduce-scatter.27.cloned.1.call-update) | async-done | bytes 32784 | tf_op jit(solution)/shard_map/reduce_scatter | solution.py:91
  198.7 20.4 %reduce-scatter.25.cloned.1.call-done = f32[16,512]{1,0:T(8,128)} async-done(((f32[64,512]{1,0:T(8,128)}), f32[16,512]{1,0:T(8,128)}) %reduce-scatter.25.cloned.1.call-update) | async-done | bytes 32784 | tf_op jit(solution)/shard_map/reduce_scatter | solution.py:90
  220.1 2.5 multiply_add_fusion
  224.6 13.1 %all_gather.14 = bf16[64,512]{1,0:T(8,128)(2,1)S(1)} all-gather(bf16[16,512]{1,0:T(8,128)(2,1)S(1)} %bitcast.26), channel_id=1, replica_groups=mesh['grp'=2,'dp'=2,'kv'=4,'tp'=2] {'kv'}, dimensions={0}, use_global_device_ids=true | all-gather | bytes 81920 | tf_op jit(solution)/shard_map/all_gather | solution.py:118
  238.8 18.4 %reduce-scatter.29.cloned.1.call-done = f32[16,1024]{1,0:T(8,128)} async-done(((f32[64,1024]{1,0:T(8,128)}), f32[16,1024]{1,0:T(8,128)}) %reduce-scatter.29.cloned.1.call-update) | async-done | bytes 65552 | tf_op jit(solution)/shard_map/reduce_scatter | solution.py:119
  258.0 5.4 %all_gather.15 = bf16[64,1024]{1,0:T(8,128)(2,1)S(1)} all-gather(bf16[16,1024]{1,0:T(8,128)(2,1)S(1)} %add_convert_fusion.1), channel_id=1, replica_groups=mesh['grp'=2,'dp'=2,'kv'=4,'tp'=2] {'dp','tp'}, dimensions={0}, use_global_device_ids=true | all-gather | bytes 163840 | tf_op jit(solution)/shard_map/all_gather | solution.py:13
  263.5 4.6 %fusion.26 = f32[64,2816]{1,0:T(8,128)} fusion(bf16[1024,2816]{1,0:T(8,128)(2,1)} %param.38, bf16[64,1024]{1,0:T(8,128)(2,1)S(1)} %all_gather.15, f32[1024]{0:T(1024)S(1)} %copy-done.8), kind=kOutput, calls=%fused_computation.47 | convolution fusion | flops 369295360 | bytes 6623232 | tf_op jit(solution)/shard_map/dot_general | solution.py:22
  268.1 4.6 %fusion.28 = f32[64,2816]{1,0:T(8,128)} fusion(bf16[1024,2816]{1,0:T(8,128)(2,1)} %param.37, bf16[64,1024]{1,0:T(8,128)(2,1)S(1)} %all_gather.15, f32[1024]{0:T(1024)S(1)} %copy-done.8), kind=kOutput, calls=%fused_computation.48 | convolution fusion | flops 369295360 | bytes 6623232 | tf_op jit(solution)/shard_map/dot_general | solution.py:21
  273.0 12.0 %all-reduce.2 = f32[64]{0:T(128)S(1)} all-reduce(f32[64]{0:T(128)S(1)} %fusion.24), channel_id=13, replica_groups=mesh['grp'=2,'dp'=2,'kv'=4,'tp'=2] {'kv'}, use_global_device_ids=true, to_apply=%region_15.17.clone | all-reduce | flops 64 | bytes 512
  285.1 6.3 %reduce-scatter.33.cloned.1.call-done = f32[16,2816]{1,0:T(8,128)} async-done(((f32[64,2816]{1,0:T(8,128)}), f32[16,2816]{1,0:T(8,128)}) %reduce-scatter.33.cloned.1.call-update) | async-done | bytes 180240 | tf_op jit(solution)/shard_map/reduce_scatter | solution.py:25
  291.4 24.3 %reduce-scatter.31.cloned.1.call-done = f32[16,2816]{1,0:T(8,128)} async-done(((f32[64,2816]{1,0:T(8,128)}), f32[16,2816]{1,0:T(8,128)}) %reduce-scatter.31.cloned.1.call-update) | async-done | bytes 180240 | tf_op jit(solution)/shard_map/reduce_scatter | solution.py:24
  316.9 6.3 %collective-permute-done.3 = bf16[16,2816]{1,0:T(8,128)(2,1)S(1)} collective-permute-done((bf16[16,2816]{1,0:T(8,128)(2,1)S(1)}, bf16[16,2816]{1,0:T(8,128)(2,1)S(1)}, u32[]{:S(2)}, u32[]{:S(2)}) %collective-permute-start.3) | collective-permute-done | bytes 90144 | tf_op jit(solution)/shard_map/ppermute | solution.py:34
  323.2 6.7 %collective-permute-done.4 = bf16[16,2816]{1,0:T(8,128)(2,1)S(1)} collective-permute-done((bf16[16,2816]{1,0:T(8,128)(2,1)S(1)}, bf16[16,2816]{1,0:T(8,128)(2,1)S(1)}, u32[]{:S(2)}, u32[]{:S(2)}) %collective-permute-start.4) | collective-permute-done | bytes 90144 | tf_op jit(solution)/shard_map/ppermute | solution.py:34
  330.0 6.3 %collective-permute-done.5 = bf16[16,2816]{1,0:T(8,128)(2,1)S(1)} collective-permute-done((bf16[16,2816]{1,0:T(8,128)(2,1)S(1)}, bf16[16,2816]{1,0:T(8,128)(2,1)S(1)}, u32[]{:S(2)}, u32[]{:S(2)}) %collective-permute-start.5) | collective-permute-done | bytes 90144 | tf_op jit(solution)/shard_map/ppermute | solution.py:34
  336.3 4.9 %fusion.4 = f32[64,1024]{1,0:T(8,128)} fusion(bf16[2816,1024]{1,0:T(8,128)(2,1)} %param.39, s32[]{:T(128)S(6)} %select_n.19, bf16[16,2816]{1,0:T(8,128)(2,1)S(1)} %collective-permute-done.5, bf16[16,2816]{1,0:T(8,128)(2,1)S(1)} %collective-permute-done.4, bf16[16,2816]{1,0:T(8,128)(2,1)S(1)} %collective-permute-done.3, ...), kind=kOutput, calls=%fused_computation.21 | convolution fusion | flops 371982336 | bytes 6389764 | tf_op jit(solution)/shard_map/dot_general | solution.py:39
  341.2 18.4 %reduce-scatter.35.cloned.1.call-done = f32[16,1024]{1,0:T(8,128)} async-done(((f32[64,1024]{1,0:T(8,128)}), f32[16,1024]{1,0:T(8,128)}) %reduce-scatter.35.cloned.1.call-update) | async-done | bytes 65552 | tf_op jit(solution)/shard_map/reduce_scatter | solution.py:38
  (82 shorter events, 19.6 us)
Async XLA Ops:
  7.2 230.6 %copy-start = (bf16[512,1024]{1,0:T(8,128)(2,1)S(1)}, bf16[512,1024]{1,0:T(8,128)(2,1)}, u32[]{:S(2)}) copy-start(bf16[512,1024]{1,0:T(8,128)(2,1)} %param.35) | copy-start | bytes 3145732
  7.2 11.6 %copy-start.7 = (f32[1024]{0:T(1024)S(1)}, f32[1024]{0:T(1024)}, u32[]{:S(2)}) copy-start(f32[1024]{0:T(1024)} %param.24) | copy-start | bytes 12292
  7.2 36.5 %reduce-scatter.15.cloned.1.call-start = ((), (), s32[]{:S(2)}) async-start(), calls=%async_computation.13 | async-start | bytes 901120 | tf_op jit(solution)/shard_map/reduce_scatter | solution.py:25
  14.1 9.4 %copy-start.10 = (u32[32]{0:T(128)S(1)}, u32[32]{0:T(128)}, u32[]{:S(2)}) copy-start(u32[32]{0:T(128)} %constant.58) | copy-start | bytes 388
  18.8 49.4 %reduce-scatter.13.cloned.1.call-start = ((), (), s32[]{:S(2)}) async-start(), calls=%async_computation.12 | async-start | bytes 901120 | tf_op jit(solution)/shard_map/reduce_scatter | solution.py:24
  23.4 88.6 %copy-start.4 = (bf16[16,1024]{1,0:T(8,128)(2,1)S(1)}, bf16[16,1024]{1,0:T(8,128)(2,1)}, u32[]{:S(2)}) copy-start(bf16[16,1024]{1,0:T(8,128)(2,1)} %param.21) | copy-start | bytes 98308
  23.4 94.8 %copy-start.5 = (f32[1024]{0:T(1024)S(1)}, f32[1024]{0:T(1024)}, u32[]{:S(2)}) copy-start(f32[1024]{0:T(1024)} %param.28) | copy-start | bytes 12292
  23.5 88.5 %reduce-scatter.17.cloned.1.call-start = ((), (), s32[]{:S(2)}) async-start(), calls=%async_computation.14 | async-start | bytes 327680 | tf_op jit(solution)/shard_map/reduce_scatter | solution.py:38
  24.9 99.2 %copy-start.2 = (bf16[1024,512]{1,0:T(8,128)(2,1)S(1)}, bf16[1024,512]{1,0:T(8,128)(2,1)}, u32[]{:S(2)}) copy-start(bf16[1024,512]{1,0:T(8,128)(2,1)} %param.32) | copy-start | bytes 3145732
  69.3 6.4 %collective-permute-start = (bf16[16,2816]{1,0:T(8,128)(2,1)S(1)}, bf16[16,2816]{1,0:T(8,128)(2,1)S(1)}, u32[]{:S(2)}, u32[]{:S(2)}) collective-permute-start(bf16[16,2816]{1,0:T(8,128)(2,1)S(1)} %multiply_convert_fusion.1), channel_id=1, source_target_pairs={{0,2},{2,4},{4,6},{6,0},{1,3},{3,5},{5,7},{7,1},{8,10},{10,12},{12... | collective-permute-start | bytes 270344 | tf_op jit(solution)/shard_map/ppermute | solution.py:34
  75.6 6.7 %collective-permute-start.1 = (bf16[16,2816]{1,0:T(8,128)(2,1)S(1)}, bf16[16,2816]{1,0:T(8,128)(2,1)S(1)}, u32[]{:S(2)}, u32[]{:S(2)}) collective-permute-start(bf16[16,2816]{1,0:T(8,128)(2,1)S(1)} %collective-permute-done), channel_id=1, source_target_pairs={{0,2},{2,4},{4,6},{6,0},{1,3},{3,5},{5,7},{7,1},{8,10},{10,12},{12... | collective-permute-start | bytes 270344 | tf_op jit(solution)/shard_map/ppermute | solution.py:34
  82.4 6.4 %collective-permute-start.2 = (bf16[16,2816]{1,0:T(8,128)(2,1)S(1)}, bf16[16,2816]{1,0:T(8,128)(2,1)}, u32[]{:S(2)}, u32[]{:S(2)}) collective-permute-start(bf16[16,2816]{1,0:T(8,128)(2,1)S(1)} %collective-permute-done.1), channel_id=1, source_target_pairs={{0,2},{2,4},{4,6},{6,0},{1,3},{3,5},{5,7},{7,1},{8,10},{10,12},{12... | collective-permute-start | bytes 270344 | tf_op jit(solution)/shard_map/ppermute | solution.py:34
  82.4 54.6 %copy-start.3 = (bf16[1024,512]{1,0:T(8,128)(2,1)S(1)}, bf16[1024,512]{1,0:T(8,128)(2,1)}, u32[]{:S(2)}) copy-start(bf16[1024,512]{1,0:T(8,128)(2,1)} %param.31) | copy-start | bytes 3145732
  82.4 96.4 %copy-start.6 = (f32[16,256]{1,0:T(8,128)S(1)}, f32[16,256]{1,0:T(8,128)}, u32[]{:S(2)}) copy-start(f32[16,256]{1,0:T(8,128)} %param.23) | copy-start | bytes 49156
  93.7 45.9 %reduce-scatter.21.cloned.1.call-start = ((), (), s32[]{:S(2)}) async-start(), calls=%async_computation.16 | async-start | bytes 81920 | tf_op jit(solution)/shard_map/reduce_scatter | solution.py:92
  120.2 104.4 %copy-start.9 = (f32[128]{0:T(128)S(1)}, f32[128]{0:T(128)}, u32[]{:S(2)}) copy-start(f32[128]{0:T(128)} %param.34) | copy-start | bytes 1540
  120.2 39.0 %reduce-scatter.23.cloned.1.call-start = ((), (), s32[]{:S(2)}) async-start(), calls=%async_computation.17 | async-start | bytes 81920 | tf_op jit(solution)/shard_map/reduce_scatter | solution.py:89
  122.1 56.7 %reduce-scatter.19.cloned.1.call-start = ((), (), s32[]{:S(2)}) async-start(), calls=%async_computation.15 | async-start | bytes 81920 | tf_op jit(solution)/shard_map/reduce_scatter | solution.py:88
  124.1 74.7 %reduce-scatter.27.cloned.1.call-start = ((), (), s32[]{:S(2)}) async-start(), calls=%async_computation.19 | async-start | bytes 163840 | tf_op jit(solution)/shard_map/reduce_scatter | solution.py:91
  125.1 138.4 %copy-start.8 = (f32[1024]{0:T(1024)S(1)}, f32[1024]{0:T(1024)}, u32[]{:S(2)}) copy-start(f32[1024]{0:T(1024)} %param.36) | copy-start | bytes 12292
  125.1 94.1 %reduce-scatter.25.cloned.1.call-start = ((), (), s32[]{:S(2)}) async-start(), calls=%async_computation.18 | async-start | bytes 163840 | tf_op jit(solution)/shard_map/reduce_scatter | solution.py:90
  138.0 119.2 %reduce-scatter.29.cloned.1.call-start = ((), (), s32[]{:S(2)}) async-start(), calls=%async_computation.20 | async-start | bytes 327680 | tf_op jit(solution)/shard_map/reduce_scatter | solution.py:119
  222.5 45.6 %copy-start.1 = (f32[16,4,64,128]{3,2,1,0:T(8,128)}, f32[16,4,64,128]{3,2,1,0:T(8,128)S(1)}, u32[]{:S(2)}) copy-start(f32[16,4,64,128]{3,2,1,0:T(8,128)S(1)} %multiply_add_fusion) | copy-start | bytes 6291460
  238.8 52.6 %reduce-scatter.33.cloned.1.call-start = ((), (), s32[]{:S(2)}) async-start(), calls=%async_computation.22 | async-start | bytes 901120 | tf_op jit(solution)/shard_map/reduce_scatter | solution.py:25
  268.1 47.6 %reduce-scatter.31.cloned.1.call-start = ((), (), s32[]{:S(2)}) async-start(), calls=%async_computation.21 | async-start | bytes 901120 | tf_op jit(solution)/shard_map/reduce_scatter | solution.py:24
  272.8 86.9 %reduce-scatter.35.cloned.1.call-start = ((), (), s32[]{:S(2)}) async-start(), calls=%async_computation.23 | async-start | bytes 327680 | tf_op jit(solution)/shard_map/reduce_scatter | solution.py:38
  316.9 6.4 %collective-permute-start.3 = (bf16[16,2816]{1,0:T(8,128)(2,1)S(1)}, bf16[16,2816]{1,0:T(8,128)(2,1)S(1)}, u32[]{:S(2)}, u32[]{:S(2)}) collective-permute-start(bf16[16,2816]{1,0:T(8,128)(2,1)S(1)} %multiply_convert_fusion), channel_id=1, source_target_pairs={{0,2},{2,4},{4,6},{6,0},{1,3},{3,5},{5,7},{7,1},{8,10},{10,12},{12... | collective-permute-start | bytes 270344 | tf_op jit(solution)/shard_map/ppermute | solution.py:34
  323.2 6.7 %collective-permute-start.4 = (bf16[16,2816]{1,0:T(8,128)(2,1)S(1)}, bf16[16,2816]{1,0:T(8,128)(2,1)S(1)}, u32[]{:S(2)}, u32[]{:S(2)}) collective-permute-start(bf16[16,2816]{1,0:T(8,128)(2,1)S(1)} %collective-permute-done.3), channel_id=1, source_target_pairs={{0,2},{2,4},{4,6},{6,0},{1,3},{3,5},{5,7},{7,1},{8,10},{10,12},{12... | collective-permute-start | bytes 270344 | tf_op jit(solution)/shard_map/ppermute | solution.py:34
  330.0 6.3 %collective-permute-start.5 = (bf16[16,2816]{1,0:T(8,128)(2,1)S(1)}, bf16[16,2816]{1,0:T(8,128)(2,1)S(1)}, u32[]{:S(2)}, u32[]{:S(2)}) collective-permute-start(bf16[16,2816]{1,0:T(8,128)(2,1)S(1)} %collective-permute-done.4), channel_id=1, source_target_pairs={{0,2},{2,4},{4,6},{6,0},{1,3},{3,5},{5,7},{7,1},{8,10},{10,12},{12... | collective-permute-start | bytes 270344 | tf_op jit(solution)/shard_map/ppermute | solution.py:34
Sparse Core Ops, SparseCore 0:
  18.9 24.7 reduce-scatter.14
  46.0 22.0 reduce-scatter.12
  93.9 18.0 reduce-scatter.16
  120.3 19.2 reduce-scatter.20
  141.7 17.4 reduce-scatter.22
  161.3 17.4 reduce-scatter.18
  181.1 17.6 reduce-scatter.26
  201.5 17.5 reduce-scatter.24
  238.9 18.2 reduce-scatter.28
  268.2 23.1 reduce-scatter.32
  293.7 21.9 reduce-scatter.30
  341.4 18.2 reduce-scatter.34
